TPU v7x, 32 devices: a whole 2x2x4 slice. The times are simulated.
32 devices in a mesh: gr: 2 (over x), fs: 8 (over z, y), tp: 2 (over core).
Axes of the slice: x: 2, y: 2, z: 4, core: 2. Of those that a mesh axis runs over, the one named last changes fastest.
Arguments:
- tokens: bfloat16 [4096, 2048], P(('gr', 'fs')), may hold values from -6 to 6
- norm_gain: float32 [2048], P(('gr', 'fs')), may hold values from 0.1 to 1.9
- gate_train: float32 [8, 2048, 1024], P(None, ('gr', 'fs'), 'tp'), may hold values from -0.125 to 0.125
- up_train: float32 [8, 2048, 1024], P(None, ('gr', 'fs'), 'tp'), may hold values from -0.125 to 0.125
- down_train: float32 [8, 1024, 2048], P(None, 'tp', ('gr', 'fs')), may hold values from -0.1875 to 0.1875
- expert_ids: int32 [4096, 2], P(('gr', 'fs')), may hold values from 0 to 7, all different within a row; in each aligned block of 256 rows (0 to 255, 256 to 511, ...) at most 128 rows name the same one
- route_score: float32 [4096, 2], P(('gr', 'fs')), may hold values from 0.05 to 1
Outputs:
- gate_ready: bfloat16 [8, 2048, 1024], P('fs', None, 'tp')
- up_ready: bfloat16 [8, 2048, 1024], P('fs', None, 'tp')
- down_ready: bfloat16 [8, 1024, 2048], P('fs', 'tp')
- mixed: bfloat16 [4096, 2048], P(('gr', 'fs'), 'tp')
Inputs may be any that keep to these rules, and one draw needn't show every extreme that they name: `expert_ids`: each row names two different experts. Among the 256 rows of one device no expert is named more than 128 times, and in every draw some expert is named exactly 128 times by some device's rows.
All inputs are finite; a program needn't handle non-finite values.
Results may differ from a plain program's by a relative error of at most 0.015.
Values may be sent and summed in bfloat16 or wider, within the bound.
A program may use at most 64 MiB of HBM per device.

v0:
```python
import jax
import jax.numpy as jnp
from jax import lax
from jax.sharding import PartitionSpec as P

epsilon = 1e-06


def shortened(shard):
    return jax.tree.map(lambda a: a.astype(jnp.bfloat16) if a.dtype == jnp.float32 else a, shard)


def move_inputs(gate_cast, up_cast):
    spread = (
        lax.all_to_all(gate_cast[:, None], "fs", split_axis=0, concat_axis=1, tiled=True),
        lax.all_to_all(up_cast[:, None], "fs", split_axis=0, concat_axis=1, tiled=True),
    )
    flattened = tuple((piece.reshape(piece.shape[0], 1, -1, piece.shape[-1]) for piece in spread))
    owned = jax.tree.map(
        lambda part, own: part.astype(own.dtype),
        lax.all_gather(shortened(flattened), "gr", axis=1, tiled=True),
        flattened,
    )
    return tuple((piece.reshape(piece.shape[0], -1, piece.shape[-1]) for piece in owned))


def move_down(down_cast):
    spread = lax.all_to_all(down_cast[:, :, None], "fs", split_axis=0, concat_axis=2, tiled=True)
    flattened = spread.reshape(spread.shape[0], spread.shape[1], 1, -1)
    owned = lax.all_gather(flattened, "gr", axis=2, tiled=True)
    return owned.reshape(owned.shape[0], owned.shape[1], -1)


def on_device(tokens, norm_gain, gate_train, up_train, down_train, expert_ids, route_score):
    gate_cast = (norm_gain[None, :, None] * gate_train).astype(jnp.bfloat16)
    up_cast = (norm_gain[None, :, None] * up_train).astype(jnp.bfloat16)
    down_cast = down_train.astype(jnp.bfloat16)
    fs_count = lax.axis_size("fs")
    experts = gate_train.shape[0]
    tok_count = tokens.shape[0]
    width = tokens.shape[1]
    capacity = 4 * tok_count // experts
    gate_ready, up_ready = move_inputs(gate_cast, up_cast)
    down_ready = move_down(down_cast)
    floated = tokens.astype(jnp.float32)
    normed = (
        floated * lax.rsqrt(jnp.mean(floated * floated, axis=-1, keepdims=True) + epsilon)
    ).astype(jnp.bfloat16)
    flat_ids = expert_ids.reshape(-1)
    matches = (flat_ids[:, None] == jnp.arange(experts, dtype=jnp.int32)[None, :]).astype(jnp.int32)
    ranked = jnp.sum((jnp.cumsum(matches, axis=0) - 1) * matches, axis=1)
    slot_index = flat_ids * capacity + ranked
    pick_token = jnp.arange(flat_ids.shape[0], dtype=jnp.int32) // 2
    slot_token = jnp.zeros((experts * capacity,), jnp.int32).at[slot_index].set(pick_token)
    filled = jnp.zeros((experts * capacity,), jnp.bool_).at[slot_index].set(True)
    gathered_rows = jnp.where(filled[:, None], normed[slot_token], jnp.zeros((), jnp.bfloat16))
    outgoing = gathered_rows.reshape(fs_count, experts // fs_count, capacity, width)
    received = lax.all_to_all(outgoing, "fs", split_axis=0, concat_axis=0, tiled=True)
    gate_act = jnp.einsum(
        "seck,ekh->sech", received, gate_ready, preferred_element_type=jnp.float32
    )
    up_act = jnp.einsum("seck,ekh->sech", received, up_ready, preferred_element_type=jnp.float32)
    hidden = (jax.nn.silu(gate_act) * up_act).astype(jnp.bfloat16)
    partial_value = jnp.einsum(
        "sech,ehk->seck", hidden, down_ready, preferred_element_type=jnp.float32
    )
    summed = lax.psum_scatter(
        partial_value.astype(jnp.bfloat16), "tp", scatter_dimension=3, tiled=True
    )
    returned = lax.all_to_all(summed, "fs", split_axis=0, concat_axis=0, tiled=True)
    flat_back = returned.reshape(experts * capacity, -1)
    picked = flat_back[slot_index].reshape(tok_count, 2, -1)
    route_share = route_score / jnp.sum(route_score, axis=-1, keepdims=True)
    mixed = jnp.sum(picked.astype(jnp.float32) * route_share[:, :, None], axis=1).astype(
        jnp.bfloat16
    )
    return (gate_ready, up_ready, down_ready, mixed)


def solution(mesh):
    return jax.shard_map(
        on_device,
        mesh=mesh,
        in_specs=(
            P(("gr", "fs"), None),
            P(("gr", "fs")),
            P(None, ("gr", "fs"), "tp"),
            P(None, ("gr", "fs"), "tp"),
            P(None, "tp", ("gr", "fs")),
            P(("gr", "fs"), None),
            P(("gr", "fs"), None),
        ),
        out_specs=(
            P("fs", None, "tp"),
            P("fs", None, "tp"),
            P("fs", "tp", None),
            P(("gr", "fs"), "tp"),
        ),
        check_vma=False,
    )
```

profile of v0, /device:TPU:0, one launch (start us, length us, event | category | flops | bytes accessed | tf_op | source)
XLA Modules:
  0.0 307.5 jit_solution(13147382898146863638)
XLA Ops:
  7.2 3.9 %fusion.16 = (bf16[8,1,128,512]{3,2,1,0:T(8,128)(2,1)}, bf16[8,1,128,512]{3,2,1,0:T(8,128)(2,1)S(1)}) fusion(f32[8,128,512]{2,1,0:T(8,128)} %param.10, f32[128]{0:T(128)} %param.8, f32[8,128,512]{2,1,0:T(8,128)} %param.9), kind=kLoop, calls=%fused_computation.26 | loop fusion | flops 2097152 | bytes 6291968 | tf_op jit(solution)/shard_map/broadcast_in_dim | solution.py:16
  11.0 0.0 copy-start.5
  11.0 33.1 %all_to_all.43 = bf16[8,1,128,512]{3,2,1,0:T(8,128)(2,1)} all-to-all(bf16[8,1,128,512]{3,2,1,0:T(8,128)(2,1)S(1)} %get-tuple-element.13), channel_id=1, replica_groups=mesh['gr'=2,'fs'=8,'tp'=2] {'fs'}, dimensions={0} | all-to-all | bytes 2097152 | tf_op jit(solution)/shard_map/all_to_all | solution.py:15
  44.1 3.6 %all-to-all-start.1 = ((bf16[8,1,128,512]{3,2,1,0:T(8,128)(2,1)}), bf16[8,1,128,512]{3,2,1,0:T(8,128)(2,1)S(1)}, u32[]{:S(2)}, u32[]{:S(2)}) async-start(bf16[8,1,128,512]{3,2,1,0:T(8,128)(2,1)} %get-tuple-element.12), calls=%async_computation.1 | async-start | bytes 2097152 | tf_op jit(solution)/shard_map/all_to_all | solution.py:16
  47.7 0.0 copy-done.5
  47.7 0.1 copy.52
  47.9 0.1 eq.29
  48.0 0.1 eq.25
  48.2 1.1 reduce-window.6
  49.3 0.2 slice_reduce_fusion
  49.6 0.1 copy.51
  49.7 0.1 mul.64
  49.9 0.0 copy-start
  49.9 2.6 copy.47
  52.5 0.1 fusion.19
  52.6 20.7 %all-to-all-done.1 = bf16[8,1,128,512]{3,2,1,0:T(8,128)(2,1)S(1)} async-done(((bf16[8,1,128,512]{3,2,1,0:T(8,128)(2,1)}), bf16[8,1,128,512]{3,2,1,0:T(8,128)(2,1)S(1)}, u32[]{:S(2)}, u32[]{:S(2)}) %all-to-all-start.1) | async-done | bytes 1048608 | tf_op jit(solution)/shard_map/all_to_all | solution.py:16
  73.3 0.0 copy-start.1
  73.3 4.3 %all-to-all-start.2 = ((bf16[8,512,1,128]{1,3,2,0:T(8,128)(2,1)}), bf16[8,512,1,128]{1,3,2,0:T(8,128)(2,1)}, u32[]{:S(2)}, u32[]{:S(2)}) async-start(bf16[8,512,1,128]{1,3,2,0:T(8,128)(2,1)} %bitcast.94), calls=%async_computation.2 | async-start | bytes 2097152 | tf_op jit(solution)/shard_map/all_to_all | solution.py:28
  77.6 2.4 scatter_custom_fusion.1
  80.0 0.0 copy-done
  80.0 0.3 fusion.4
  80.3 0.2 fusion.5
  80.6 0.0 copy-done.1
  80.6 6.0 %gather_fusion = bf16[1024,2048]{1,0:T(8,128)(2,1)} fusion(bf16[256,2048]{1,0:T(8,128)(2,1)S(1)} %fusion.5, s32[1024]{0:T(1024)S(1)} %fusion.21), kind=kCustom, calls=%fused_computation | custom fusion | bytes 8392704 | tf_op jit(solution)/shard_map/gather | solution.py:56
  86.6 2.4 scatter_custom_fusion
  89.1 4.5 %broadcast_select_fusion = bf16[8,1,128,2048]{3,2,1,0:T(8,128)(2,1)} fusion(bf16[8,1,128,2048]{3,2,1,0:T(8,128)(2,1)} %bitcast.99, pred[8,128]{1,0:T(8,128)(4,1)S(1)} %bitcast.112), kind=kLoop, calls=%fused_computation.9 | loop fusion | flops 2097152 | bytes 8389632 | tf_op jit(solution)/shard_map/jit(_where)/select_n | solution.py:56
  93.6 9.4 %all-to-all-done.2 = bf16[8,512,1,128]{1,3,2,0:T(8,128)(2,1)} async-done(((bf16[8,512,1,128]{1,3,2,0:T(8,128)(2,1)}), bf16[8,512,1,128]{1,3,2,0:T(8,128)(2,1)}, u32[]{:S(2)}, u32[]{:S(2)}) %all-to-all-start.2) | async-done | bytes 1048608 | tf_op jit(solution)/shard_map/all_to_all | solution.py:28
  103.0 4.5 %all-to-all-start.3 = ((bf16[8,1,128,2048]{3,2,1,0:T(8,128)(2,1)}), bf16[8,1,128,2048]{3,2,1,0:T(8,128)(2,1)}, u32[]{:S(2)}, u32[]{:S(2)}) async-start(bf16[8,1,128,2048]{3,2,1,0:T(8,128)(2,1)} %broadcast_select_fusion), calls=%async_computation.3 | async-start | bytes 8388608 | tf_op jit(solution)/shard_map/all_to_all | solution.py:58
  107.6 0.0 all-gather.8.cloned.1.call-start
  107.6 2.3 copy.48
  109.9 0.0 all-gather.8.cloned.1.call-update
  109.9 0.0 all-gather.4.cloned.1.call-start
  109.9 0.7 all-gather.4.cloned.1.call-update
  110.7 0.0 all-gather.6.cloned.1.call-start
  110.7 0.7 all-gather.6.cloned.1.call-update
  111.4 0.2 reduce-scatter.2.cloned.1.call-start
  111.6 33.3 %all-gather.8.cloned.1.call-done = bf16[1,512,2,1024]{3,1,0,2:T(8,128)(2,1)} async-done(((bf16[1,512,1,1024]{3,1,0,2:T(8,128)(2,1)}), bf16[1,512,2,1024]{3,1,0,2:T(8,128)(2,1)}) %all-gather.8.cloned.1.call-update) | async-done | bytes 2097168 | tf_op jit(solution)/shard_map/all_gather | solution.py:30
  144.9 3.7 %copy.56 = bf16[1,512,2,1024]{3,2,1,0:T(2,128)(2,1)S(1)} copy(bf16[1,512,2,1024]{3,1,0,2:T(8,128)(2,1)} %all-gather.8.cloned.1.call-done) | data formatting | bytes 4194304 | tf_op jit(solution)/shard_map/all_gather | solution.py:30
  148.7 2.8 reshape.191
  151.5 28.1 %all-gather.4.cloned.1.call-done = bf16[1,2,1024,512]{3,2,0,1:T(8,128)(2,1)} async-done(((bf16[1,1,1024,512]{3,2,0,1:T(8,128)(2,1)}), bf16[1,2,1024,512]{3,2,0,1:T(8,128)(2,1)}) %all-gather.4.cloned.1.call-update) | async-done | bytes 2097168 | tf_op jit(solution)/shard_map/all_gather | solution.py:21
  179.6 20.3 %all-to-all-done.3 = bf16[8,1,128,2048]{3,2,1,0:T(8,128)(2,1)} async-done(((bf16[8,1,128,2048]{3,2,1,0:T(8,128)(2,1)}), bf16[8,1,128,2048]{3,2,1,0:T(8,128)(2,1)}, u32[]{:S(2)}, u32[]{:S(2)}) %all-to-all-start.3) | async-done | bytes 4194336 | tf_op jit(solution)/shard_map/all_to_all | solution.py:58
  199.8 0.0 copy-start.4
  199.8 6.7 %fusion.2 = f32[512,8,128]{2,0,1:T(8,128)} fusion(bf16[2048,512,1]{1,0,2:T(8,128)(2,1)} %bitcast.103, bf16[8,1,128,2048]{3,2,1,0:T(8,128)(2,1)} %all-to-all-done.3), kind=kOutput, calls=%fused_computation.6 | convolution fusion | flops 2147483648 | bytes 8388608 | tf_op jit(solution)/shard_map/seck,ekh->sech/dot_general | solution.py:59
  206.5 8.3 %all-gather.6.cloned.1.call-done = bf16[1,2,1024,512]{3,2,0,1:T(8,128)(2,1)} async-done(((bf16[1,1,1024,512]{3,2,0,1:T(8,128)(2,1)}), bf16[1,2,1024,512]{3,2,0,1:T(8,128)(2,1)}) %all-gather.6.cloned.1.call-update) | async-done | bytes 2097168 | tf_op jit(solution)/shard_map/all_gather | solution.py:21
  214.8 0.0 copy-done.4
  214.8 8.9 %convert_bitcast_fusion = bf16[8,1,128,2048]{3,2,0,1:T(8,128)(2,1)} fusion(bf16[512,2048,1]{1,0,2:T(8,128)(2,1)S(1)} %copy-done.4, bf16[2048,512,1]{1,0,2:T(8,128)(2,1)} %bitcast.105, bf16[8,1,128,2048]{3,2,1,0:T(8,128)(2,1)} %all-to-all-done.3, f32[512,8,128]{2,0,1:T(8,128)} %fusion.2), kind=kOutput, calls=%fused_computation.8 | convolution fusion | flops 4300210176 | bytes 14680064 | tf_op jit(solution)/shard_map/sech,ehk->seck/dot_general | solution.py:64
  223.8 0.0 reduce-scatter.2.cloned.1.call-update
  223.8 12.0 %reduce-scatter.2.cloned.1.call-done = bf16[8,1,128,1024]{3,2,0,1:T(8,128)(2,1)} async-done(((bf16[8,1,128,2048]{3,2,0,1:T(8,128)(2,1)}), bf16[8,1,128,1024]{3,2,0,1:T(8,128)(2,1)}) %reduce-scatter.2.cloned.1.call-update) | async-done | bytes 2097168 | tf_op jit(solution)/shard_map/reduce_scatter | solution.py:67
  235.8 0.0 copy-start.6
  235.8 6.0 %all-to-all-start.4 = ((bf16[8,1,128,1024]{3,2,1,0:T(8,128)(2,1)}), bf16[8,1,128,1024]{3,2,1,0:T(8,128)(2,1)S(1)}, u32[]{:S(2)}, u32[]{:S(2)}) async-start(bf16[8,1,128,1024]{3,2,1,0:T(8,128)(2,1)} %bitcast.107), calls=%async_computation.5 | async-start | bytes 4194304 | tf_op jit(solution)/shard_map/all_to_all | solution.py:70
  241.8 0.0 copy-done.6
  241.9 0.1 copy.59
  242.0 3.9 %copy.49 = bf16[1,512,2,1024]{1,3,2,0:T(8,128)(2,1)} copy(bf16[1,512,2,1024]{3,1,0,2:T(8,128)(2,1)} %all-gather.8.cloned.1.call-done) | data formatting | bytes 4194304 | tf_op jit(solution)/shard_map/all_gather | solution.py:30
  246.0 3.9 %copy.60 = bf16[1,512,2048]{2,1,0:T(8,128)(2,1)} copy(bf16[1,512,2048]{1,2,0:T(8,128)(2,1)} %bitcast.100) | data formatting | bytes 4194304
  249.9 40.5 %all-to-all-done.4 = bf16[8,1,128,1024]{3,2,1,0:T(8,128)(2,1)S(1)} async-done(((bf16[8,1,128,1024]{3,2,1,0:T(8,128)(2,1)}), bf16[8,1,128,1024]{3,2,1,0:T(8,128)(2,1)S(1)}, u32[]{:S(2)}, u32[]{:S(2)}) %all-to-all-start.4) | async-done | bytes 2097184 | tf_op jit(solution)/shard_map/all_to_all | solution.py:70
  290.4 2.0 gather_fusion.1
  292.5 1.3 reshape.155
  293.8 0.0 copy-start.2
  293.8 3.5 %multiply_reduce_fusion = bf16[256,1024]{1,0:T(8,128)(2,1)} fusion(f32[256,2,1024]{2,1,0:T(2,128)S(1)} %reshape.155, f32[256,2]{1,0:T(8,128)S(1)} %copy.59), kind=kLoop, calls=%fused_computation.21 | loop fusion | flops 786432 | bytes 2623488 | tf_op jit(solution)/shard_map/reduce_sum | solution.py:74
  297.3 0.0 copy-done.2
  297.3 0.0 copy-start.3
  297.3 1.3 copy.66
  298.6 1.0 copy-done.3
  299.7 1.3 copy.67
  (12 shorter events, 0.1 us)
Async XLA Ops:
  11.0 36.7 %copy-start.5 = (s32[256,2]{0,1:T(2,128)S(1)}, s32[256,2]{0,1:T(2,128)}, u32[]{:S(2)}) copy-start(s32[256,2]{0,1:T(2,128)} %param.12) | copy-start | bytes 6148
  44.1 29.2 %all-to-all-start.1 = ((bf16[8,1,128,512]{3,2,1,0:T(8,128)(2,1)}), bf16[8,1,128,512]{3,2,1,0:T(8,128)(2,1)S(1)}, u32[]{:S(2)}, u32[]{:S(2)}) async-start(bf16[8,1,128,512]{3,2,1,0:T(8,128)(2,1)} %get-tuple-element.12), calls=%async_computation.1 | async-start | bytes 2097152 | tf_op jit(solution)/shard_map/all_to_all | solution.py:16
  49.9 30.1 %copy-start = (bf16[256,2048]{1,0:T(8,128)(2,1)S(1)}, bf16[256,2048]{1,0:T(8,128)(2,1)}, u32[]{:S(2)}) copy-start(bf16[256,2048]{1,0:T(8,128)(2,1)} %param.7) | copy-start | bytes 3145732
  73.3 7.3 %copy-start.1 = (bf16[8,1,128,512]{3,2,1,0:T(8,128)(2,1)}, bf16[8,1,128,512]{3,2,1,0:T(8,128)(2,1)S(1)}, u32[]{:S(2)}) copy-start(bf16[8,1,128,512]{3,2,1,0:T(8,128)(2,1)S(1)} %all-to-all-done.1) | copy-start | bytes 3145732
  73.3 29.7 %all-to-all-start.2 = ((bf16[8,512,1,128]{1,3,2,0:T(8,128)(2,1)}), bf16[8,512,1,128]{1,3,2,0:T(8,128)(2,1)}, u32[]{:S(2)}, u32[]{:S(2)}) async-start(bf16[8,512,1,128]{1,3,2,0:T(8,128)(2,1)} %bitcast.94), calls=%async_computation.2 | async-start | bytes 2097152 | tf_op jit(solution)/shard_map/all_to_all | solution.py:28
  103.0 96.8 %all-to-all-start.3 = ((bf16[8,1,128,2048]{3,2,1,0:T(8,128)(2,1)}), bf16[8,1,128,2048]{3,2,1,0:T(8,128)(2,1)}, u32[]{:S(2)}, u32[]{:S(2)}) async-start(bf16[8,1,128,2048]{3,2,1,0:T(8,128)(2,1)} %broadcast_select_fusion), calls=%async_computation.3 | async-start | bytes 8388608 | tf_op jit(solution)/shard_map/all_to_all | solution.py:58
  107.6 37.4 %all-gather.8.cloned.1.call-start = ((), (), s32[]{:S(2)}) async-start(), calls=%async_computation.8 | async-start | bytes 3145728 | tf_op jit(solution)/shard_map/all_gather | solution.py:30
  109.9 69.7 %all-gather.4.cloned.1.call-start = ((), (), s32[]{:S(2)}) async-start(), calls=%async_computation.6 | async-start | bytes 3145728 | tf_op jit(solution)/shard_map/all_gather | solution.py:21
  110.7 104.2 %all-gather.6.cloned.1.call-start = ((), (), s32[]{:S(2)}) async-start(), calls=%async_computation.7 | async-start | bytes 3145728 | tf_op jit(solution)/shard_map/all_gather | solution.py:21
  111.4 124.4 %reduce-scatter.2.cloned.1.call-start = ((), (), s32[]{:S(2)}) async-start(), calls=%async_computation.9 | async-start | bytes 6291456 | tf_op jit(solution)/shard_map/reduce_scatter | solution.py:67
  199.8 15.0 %copy-start.4 = (bf16[512,2048,1]{1,0,2:T(8,128)(2,1)S(1)}, bf16[512,2048,1]{1,0,2:T(8,128)(2,1)}, u32[]{:S(2)}) copy-start(bf16[512,2048,1]{1,0,2:T(8,128)(2,1)} %reshape.191) | copy-start | bytes 6291460
  235.8 6.0 %copy-start.6 = (f32[256,2]{0,1:T(2,128)S(1)}, f32[256,2]{0,1:T(2,128)}, u32[]{:S(2)}) copy-start(f32[256,2]{0,1:T(2,128)} %param.13) | copy-start | bytes 6148
  235.8 54.6 %all-to-all-start.4 = ((bf16[8,1,128,1024]{3,2,1,0:T(8,128)(2,1)}), bf16[8,1,128,1024]{3,2,1,0:T(8,128)(2,1)S(1)}, u32[]{:S(2)}, u32[]{:S(2)}) async-start(bf16[8,1,128,1024]{3,2,1,0:T(8,128)(2,1)} %bitcast.107), calls=%async_computation.5 | async-start | bytes 4194304 | tf_op jit(solution)/shard_map/all_to_all | solution.py:70
  293.8 3.5 %copy-start.2 = (bf16[1,2,1024,512]{3,2,0,1:T(8,128)(2,1)S(1)}, bf16[1,2,1024,512]{3,2,0,1:T(8,128)(2,1)}, u32[]{:S(2)}) copy-start(bf16[1,2,1024,512]{3,2,0,1:T(8,128)(2,1)} %all-gather.4.cloned.1.call-done) | copy-start | bytes 6291460
  297.3 2.3 copy-start.3
Sparse Core Ops, SparseCore 0:
  110.5 34.3 all-gather.7
  146.5 33.0 all-gather.3
  181.7 33.0 all-gather.5
  223.9 11.8 reduce-scatter.1
where the time goes:
time: 308 us
  waiting for transfers between devices  174 us (56%)
  local copies, waits for them, and re-layouts  38.3 us (12%)
  blocking collectives  33.1 us (11%)
  starting transfers between devices  18.7 us (6%)
  matrix products  15.6 us (5%)
  between operations  13.9 us (5%)
  other arithmetic  13.7 us (4%)
    all_to_all x1, waiting for transfers between devices, on_device(): lax.all_to_all(summed, 'fs', split_axis=0, concat_axis=0, tiled=True)  40.5 us
    all_gather x2, waiting for transfers between devices, move_inputs(): lax.all_gather(shortened(flattened), 'gr', axis=1, tiled=True)  36.4 us
    all_gather x1, waiting for transfers between devices, move_down(): owned = lax.all_gather(flattened, 'gr', axis=2, tiled=True)  33.3 us
    all_to_all x1, blocking collectives, move_inputs(): lax.all_to_all(gate_cast[:, None], 'fs', split_axis=0, concat_axis=1, til...  33.1 us
    all_to_all x1, waiting for transfers between devices, move_inputs(): lax.all_to_all(up_cast[:, None], 'fs', split_axis=0, concat_axis=1, tiled...  20.7 us
    all_to_all x1, waiting for transfers between devices, on_device(): lax.all_to_all(outgoing, 'fs', split_axis=0, concat_axis=0, tiled=True)  20.3 us
    reduce_scatter x1, waiting for transfers between devices, on_device(): lax.psum_scatter(partial_value.astype(jnp.bfloat16), 'tp', scatter_dimens...  12 us
    unnamed x19, local copies, waits for them, and re-layouts  10.4 us
  transfers between devices with their start and end apart: 8, of which 8 were waited for; matrix products, arithmetic and copies ran while one was open for 14% of the time, Pallas kernels for 0%

commit v1 on v0

v1 whole, which is shorter than its diff:
```python
import functools

import jax
import jax.numpy as jnp
from jax import lax
from jax.experimental import pallas as pl
from jax.experimental.pallas import tpu as pltpu
from jax.sharding import PartitionSpec as P

epsilon = 1e-06
MESH = pl.DeviceIdType.MESH


def remote(src, dst, send_sem, recv_sem, where):
    return pltpu.make_async_remote_copy(
        src_ref=src, dst_ref=dst, send_sem=send_sem, recv_sem=recv_sem, device_id=where, device_id_type=MESH
    )


def greet(sizes):
    barrier = pltpu.get_barrier_semaphore()
    count = 0
    for name, size in sizes.items():
        me = lax.axis_index(name)
        for k in range(1, size):
            pl.semaphore_signal(barrier, inc=1, device_id={name: lax.rem(me + k, size)}, device_id_type=MESH)
            count += 1
    pl.semaphore_wait(barrier, count)


def spread_kernel(sizes, local, direct_down, gate, up, down, rows, keys, gate_out, up_out, down_out, rows_out, keys_out,
                  w_send, w_recv, g_send, g_recv, up_send, low_send, y_send, x_recv, t_send, t_recv, k_send, k_recv, own_sem):
    n_gr, n_fs, n_tp = sizes["gr"], sizes["fs"], sizes["tp"]
    g, f, p = lax.axis_index("gr"), lax.axis_index("fs"), lax.axis_index("tp")
    inner = 2 if n_fs % 2 == 0 else 1
    lines = n_fs // inner
    z, y = f // inner, lax.rem(f, inner)
    depth = gate.shape[1]
    half = rows.shape[1] // n_tp
    cols = pl.ds(pl.multiple_of(p * half, half), half)
    sources, outs = (gate, up, down), (gate_out, up_out, down_out)

    def place(w, block):
        start = pl.multiple_of(block * depth, depth)
        if w < 2:
            return outs[w].at[:, pl.ds(start, depth), :]
        return outs[w].at[:, :, pl.ds(start, depth)] if direct_down else outs[w].at[block]

    greet(sizes)

    own = [pltpu.make_async_copy(rows, rows_out.at[f], own_sem.at[0]),
           pltpu.make_async_copy(keys, keys_out.at[f], own_sem.at[1])]
    for w in range(3):
        own.append(pltpu.make_async_copy(sources[w].at[pl.ds(f * local, local)], place(w, g * n_fs + f), own_sem.at[2 + w]))

    def block_of(b):
        return rows_out.at[b, :, cols]

    def row_copy(b, first, kind, where):
        src = rows.at[:, cols] if first else block_of(b)
        return remote(src, block_of(b), {"u": up_send, "d": low_send, "y": y_send}[kind].at[b], x_recv.at[b], where)

    def tp_copy(b, j):
        return remote(block_of(b), block_of(b), t_send.at[j, b], t_recv.at[j, b], {"tp": lax.rem(p + j + 1, n_tp)})

    def go_up(b, first, act):
        @pl.when(z < lines - 1)
        def _():
            act(row_copy(b, first, "u", {"fs": lax.rem(f + inner, n_fs)}))

    def go_down(b, first, act):
        @pl.when(z > 0)
        def _():
            act(row_copy(b, first, "d", {"fs": lax.rem(f + n_fs - inner, n_fs)}))

    def go_side(b, first, act):
        if inner == 2:
            act(row_copy(b, first, "y", {"fs": f + 1 - 2 * y}))

    def start(c):
        c.start()

    def recv(c):
        c.wait_recv()

    def sent(c):
        c.wait_send()

    go_up(f, True, start)
    go_down(f, True, start)
    go_side(f, True, start)
    key_copies = []
    for k in range(1, n_fs):
        to = lax.rem(f + k, n_fs)
        c = remote(keys, keys_out.at[f], k_send.at[k], k_recv.at[k], {"fs": to})
        c.start()
        key_copies.append(c)
    for c in own:
        c.start()

    def gr_copy(w, b, k, j, first):
        src = sources[w].at[pl.ds(f * local, local)] if first else place(w, b)
        return remote(src, place(w, b), g_send.at[w, k, j], g_recv.at[w, k, j], {"gr": lax.rem(g + j + 1, n_gr)})

    for w in range(3):
        for j in range(n_gr - 1):
            gr_copy(w, g * n_fs + f, 0, j, True).start()

    for s in range(1, lines):
        @pl.when(z >= s)
        def _():
            b = f - s * inner
            row_copy(b, False, "u", {"fs": lax.rem(f + inner, n_fs)}).wait_recv()
            go_up(b, False, start)
            go_side(b, False, start)
            for j in range(n_tp - 1):
                tp_copy(b, j).start()

        @pl.when(z < lines - s)
        def _():
            b = f + s * inner
            row_copy(b, False, "d", {"fs": lax.rem(f + inner, n_fs)}).wait_recv()
            go_down(b, False, start)
            go_side(b, False, start)
            for j in range(n_tp - 1):
                tp_copy(b, j).start()

    def w_copy(w, k):
        to = lax.rem(f + k, n_fs)
        return remote(sources[w].at[pl.ds(to * local, local)], place(w, g * n_fs + f), w_send.at[w, k], w_recv.at[w, k], {"fs": to})

    for w in range(3):
        for k in range(1, n_fs):
            w_copy(w, k).start()

    if inner == 2:
        for s in range(lines):
            b = lax.rem(z + s, lines) * inner + 1 - y
            row_copy(b, False, "y", {"fs": f + 1 - 2 * y}).wait_recv()
            for j in range(n_tp - 1):
                tp_copy(b, j).start()

    for w in range(3):
        for k in range(1, n_fs):
            w_copy(w, k).wait_recv()
            b = g * n_fs + lax.rem(f + n_fs - k, n_fs)
            for j in range(n_gr - 1):
                gr_copy(w, b, k, j, False).start()

    for k in range(1, n_fs):
        b = lax.rem(f + k, n_fs)
        for j in range(n_tp - 1):
            c = tp_copy(b, j)
            c.wait_recv()
            c.wait_send()
    for c in key_copies:
        c.wait_recv()
        c.wait_send()
    for c in own:
        c.wait()
    go_up(f, True, sent)
    go_down(f, True, sent)
    go_side(f, True, sent)
    for s in range(1, lines):
        @pl.when(z >= s)
        def _():
            go_up(f - s * inner, False, sent)
            go_side(f - s * inner, False, sent)

        @pl.when(z < lines - s)
        def _():
            go_down(f + s * inner, False, sent)
            go_side(f + s * inner, False, sent)
    for w in range(3):
        for k in range(n_fs):
            if k:
                w_copy(w, k).wait_send()
            for j in range(n_gr - 1):
                c = gr_copy(w, g * n_fs + lax.rem(f + n_fs - k, n_fs), k, j, False)
                c.wait_recv()
                c.wait_send()


def return_kernel(sizes, part, out, held, total, t_send, t_recv, f_send, f_recv):
    n_fs, n_tp = sizes["fs"], sizes["tp"]
    f, p = lax.axis_index("fs"), lax.axis_index("tp")
    half = part.shape[2] // n_tp

    def cols(q):
        return pl.ds(pl.multiple_of(q * half, half), half)

    greet({"fs": n_fs, "tp": n_tp})
    order = list(range(1, n_fs)) + [0]

    def tp_copy(k, j):
        to = lax.rem(p + j + 1, n_tp)
        b = lax.rem(f + k, n_fs)
        return remote(part.at[b, :, cols(to)], held.at[j, b], t_send.at[j, k], t_recv.at[j, k], {"tp": to})

    def f_copy(k):
        b = lax.rem(f + k, n_fs)
        return remote(total.at[b], out.at[f], f_send.at[k], f_recv.at[k], {"fs": b})

    for k in order:
        for j in range(n_tp - 1):
            tp_copy(k, j).start()
    for k in order:
        b = lax.rem(f + k, n_fs)
        value = part[b, :, cols(p)].astype(jnp.float32)
        for j in range(n_tp - 1):
            tp_copy(k, j).wait_recv()
            value = value + held[j, b].astype(jnp.float32)
        value = value.astype(jnp.bfloat16)
        if k == 0:
            out[b] = value
        else:
            total[b] = value
            f_copy(k).start()
    for k in order:
        for j in range(n_tp - 1):
            tp_copy(k, j).wait_send()
        if k:
            f_copy(k).wait_recv()
            f_copy(k).wait_send()


def on_device(sizes, tokens, norm_gain, gate_train, up_train, down_train, expert_ids, route_score):
    n_gr, n_fs, n_tp = sizes["gr"], sizes["fs"], sizes["tp"]
    bf16 = jnp.bfloat16
    experts, depth, hid = gate_train.shape
    local = experts // n_fs
    count, width = tokens.shape
    capacity = 4 * count // experts
    gate_cast = (norm_gain[None, :, None] * gate_train).astype(bf16)
    up_cast = (norm_gain[None, :, None] * up_train).astype(bf16)
    down_cast = down_train.astype(bf16)
    floated = tokens.astype(jnp.float32)
    normed = (floated * lax.rsqrt(jnp.mean(floated * floated, axis=-1, keepdims=True) + epsilon)).astype(bf16)

    named = expert_ids[:, :, None] == jnp.arange(experts, dtype=jnp.int32)
    names = jnp.any(named, axis=1)
    earlier = jnp.arange(count)[:, None] > jnp.arange(count)[None, :]
    rank = jnp.dot(earlier.astype(bf16), names.astype(bf16), preferred_element_type=jnp.float32).astype(jnp.int32)
    slot = expert_ids * capacity + jnp.sum(jnp.where(named, rank[:, None, :], 0), axis=2)
    keys = jnp.concatenate([slot.T, jnp.full((6, count), -1, jnp.int32)], axis=0)

    direct_down = depth % 128 == 0
    down_shape = (local, hid, n_gr * n_fs * depth) if direct_down else (n_gr * n_fs, local, hid, depth)
    dma = pltpu.SemaphoreType.DMA
    gate_ready, up_ready, down_ready, gathered, all_keys = pl.pallas_call(
        functools.partial(spread_kernel, sizes, local, direct_down),
        out_shape=(
            jax.ShapeDtypeStruct((local, n_gr * n_fs * depth, hid), bf16),
            jax.ShapeDtypeStruct((local, n_gr * n_fs * depth, hid), bf16),
            jax.ShapeDtypeStruct(down_shape, bf16),
            jax.ShapeDtypeStruct((n_fs, count, width), bf16),
            jax.ShapeDtypeStruct((n_fs, 8, count), jnp.int32),
        ),
        in_specs=[pl.BlockSpec(memory_space=pltpu.VMEM)] * 5,
        out_specs=[pl.BlockSpec(memory_space=pl.ANY)] * 5,
        scratch_shapes=[
            dma((3, n_fs)), dma((3, n_fs)), dma((3, n_fs, n_gr)), dma((3, n_fs, n_gr)),
            dma((n_fs,)), dma((n_fs,)), dma((n_fs,)), dma((n_fs,)),
            dma((n_tp, n_fs)), dma((n_tp, n_fs)), dma((n_fs,)), dma((n_fs,)), dma((5,)),
        ],
        compiler_params=pltpu.CompilerParams(collective_id=0, has_side_effects=True),
        name="spread",
    )(gate_cast, up_cast, down_cast, normed, keys)
    if not direct_down:
        down_ready = down_ready.transpose(1, 2, 0, 3).reshape(local, hid, -1)

    wanted = (lax.axis_index("fs") * local * capacity + jnp.arange(local * capacity, dtype=jnp.int32))[None, :, None]
    pick = ((all_keys[:, 0][:, None, :] == wanted) | (all_keys[:, 1][:, None, :] == wanted)).astype(bf16)
    rows = jnp.einsum("sct,std->scd", pick, gathered, preferred_element_type=jnp.float32).astype(bf16)
    rows = rows.reshape(n_fs, local, capacity, width)
    gate_act = jnp.einsum("seck,ekh->sech", rows, gate_ready, preferred_element_type=jnp.float32)
    up_act = jnp.einsum("seck,ekh->sech", rows, up_ready, preferred_element_type=jnp.float32)
    hidden = (jax.nn.silu(gate_act) * up_act).astype(bf16)
    part = jnp.einsum("sech,ehk->seck", hidden, down_ready, preferred_element_type=jnp.float32).astype(bf16)
    part = part.reshape(n_fs, local * capacity, width)
    half = width // n_tp
    returned = pl.pallas_call(
        functools.partial(return_kernel, sizes),
        out_shape=jax.ShapeDtypeStruct((n_fs, local * capacity, half), bf16),
        in_specs=[pl.BlockSpec(memory_space=pltpu.VMEM)],
        out_specs=pl.BlockSpec(memory_space=pltpu.VMEM),
        scratch_shapes=[
            pltpu.VMEM((max(n_tp - 1, 1), n_fs, local * capacity, half), bf16),
            pltpu.VMEM((n_fs, local * capacity, half), bf16),
            dma((n_tp, n_fs)), dma((n_tp, n_fs)), dma((n_fs,)), dma((n_fs,)),
        ],
        compiler_params=pltpu.CompilerParams(collective_id=1, has_side_effects=True),
        name="giveback",
    )(part)
    share = route_score / jnp.sum(route_score, axis=-1, keepdims=True)
    at = jnp.arange(experts * capacity, dtype=jnp.int32)[None, :]
    weight = jnp.where(slot[:, :1] == at, share[:, :1], 0.0) + jnp.where(slot[:, 1:] == at, share[:, 1:], 0.0)
    mixed = jnp.dot(weight.astype(bf16), returned.reshape(experts * capacity, half), preferred_element_type=jnp.float32)
    return gate_ready, up_ready, down_ready, mixed.astype(bf16)


def solution(mesh):
    return jax.shard_map(
        functools.partial(on_device, dict(mesh.shape)),
        mesh=mesh,
        in_specs=(
            P(("gr", "fs"), None),
            P(("gr", "fs")),
            P(None, ("gr", "fs"), "tp"),
            P(None, ("gr", "fs"), "tp"),
            P(None, "tp", ("gr", "fs")),
            P(("gr", "fs"), None),
            P(("gr", "fs"), None),
        ),
        out_specs=(
            P("fs", None, "tp"),
            P("fs", None, "tp"),
            P("fs", "tp", None),
            P(("gr", "fs"), "tp"),
        ),
        check_vma=False,
    )
```

time: 308 us -> 229 us (0.74)
  the two profiles are of different devices: /device:TPU:0 before, /device:TPU:13 now
where the time goes in v1:
time: 229 us
  Pallas kernels  196 us (86%)
  matrix products  17.9 us (8%)
  other arithmetic  7.07 us (3%)
  local copies, waits for them, and re-layouts  6.57 us (3%)
    pallas_call x1, Pallas kernels, on_device(): pl.pallas_call(functools.partial(spread_kernel, sizes, local, direct_down...  118 us
    pallas_call x1, Pallas kernels, on_device(): pl.pallas_call(functools.partial(return_kernel, sizes), out_shape=jax.Sha...  78.4 us
    unnamed x22, local copies, waits for them, and re-layouts  5.02 us
    dot_general x1, matrix products, on_device(): jnp.einsum('sct,std->scd', pick, gathered, preferred_element_type=jnp.flo...  4.83 us

profile of v1, /device:TPU:13, one launch (start us, length us, event | category | flops | bytes accessed | tf_op | source)
XLA Modules:
  0.0 228.8 jit_solution(9720584921683602503)
XLA Ops:
  0.6 0.0 copy-start.7
  0.6 0.0 copy-start
  0.7 4.3 %multiply_convert_fusion = (bf16[8,128,512]{2,1,0:T(8,128)(2,1)}, bf16[8,128,512]{2,1,0:T(8,128)(2,1)}) fusion(f32[8,128,512]{2,1,0:T(8,128)} %param.10, f32[128]{0:T(128)} %param.8, f32[8,128,512]{2,1,0:T(8,128)} %param.9), kind=kLoop, calls=%fused_computation.18 | loop fusion | flops 2097152 | bytes 6291968 | tf_op jit(solution)/shard_map/convert_element_type | solution.py:235
  5.0 0.0 copy-start.1
  5.0 0.0 copy-done.7
  5.0 0.2 convolution_convert_fusion.2
  5.2 0.6 concatenate.3.keys
  5.8 0.0 copy-done
  5.8 0.3 fusion
  6.1 1.2 fusion.1.rows
  7.3 0.0 copy-done.1
  7.3 1.1 convert_element_type.44.down
  8.5 118.1 %spread.1 = (bf16[1,2048,512]{2,1,0:T(8,128)(2,1)}, bf16[1,2048,512]{2,1,0:T(8,128)(2,1)}, bf16[1,512,2048]{2,1,0:T(8,128)(2,1)}, bf16[8,256,2048]{2,1,0:T(8,128)(2,1)}, s32[8,8,256]{2,1,0:T(8,128)}) custom-call(bf16[8,128,512]{2,1,0:T(8,128)(2,1)} %get-tuple-element.21.gate, bf16[8,128,512]{2,1,0:T(8,128)(2,1)} %get-tuple-element.20.up, ...), custom_call_target="tpu_custom_call" | custom-call | tf_op jit(solution)/shard_map/spread/pallas_call | solution.py:250
  126.6 0.9 fusion.29
  127.6 0.0 copy-start.3
  127.6 4.8 %convolution_convert_fusion = bf16[8,128,2048]{2,1,0:T(8,128)(2,1)S(1)} fusion(bf16[8,256,2048]{2,1,0:T(8,128)(2,1)} %get-tuple-element.13, s32[8,256]{1,0:T(8,128)S(1)} %get-tuple-element.22, s32[8,256]{1,0:T(8,128)S(1)} %get-tuple-element.23, s32[128]{0:T(128)S(1)} %iota_add_fusion), kind=kOutput, calls=%fused_computation.1 | convolution fusion | flops 1076625408 | bytes 12599808 | tf_op jit(solution)/shard_map/sct,std->scd/dot_general | solution.py:274
  132.4 0.0 copy-done.3
  132.4 0.0 copy-start.5
  132.4 2.4 %fusion.3 = f32[512,8,128]{2,0,1:T(8,128)S(1)} fusion(bf16[8,128,2048]{2,1,0:T(8,128)(2,1)S(1)} %convolution_convert_fusion, bf16[1,2048,512]{2,1,0:T(8,128)(2,1)S(1)} %copy-done.3), kind=kOutput, calls=%fused_computation.8 | convolution fusion | flops 2147483648 | bytes 8388608 | tf_op jit(solution)/shard_map/seck,ekh->sech/dot_general | solution.py:277
  134.8 0.0 copy-done.5
  134.8 0.0 copy-start.2
  134.8 2.8 %fusion.13 = bf16[8,128,512]{1,2,0:T(8,128)(2,1)S(1)} fusion(f32[512,8,128]{2,0,1:T(8,128)S(1)} %fusion.3, bf16[8,128,2048]{2,1,0:T(8,128)(2,1)S(1)} %convolution_convert_fusion, bf16[1,2048,512]{2,1,0:T(8,128)(2,1)S(1)} %copy-done.5), kind=kOutput, calls=%fused_computation.20 | convolution fusion | flops 2150629376 | bytes 9437184 | tf_op jit(solution)/shard_map/seck,ekh->sech/dot_general | solution.py:276
  137.6 0.0 copy-done.2
  137.7 4.3 %convert_bitcast_fusion.part = bf16[8,128,2048]{2,1,0:T(8,128)(2,1)} fusion(bf16[8,128,512]{1,2,0:T(8,128)(2,1)S(1)} %fusion.13, bf16[1,512,2048]{2,1,0:T(8,128)(2,1)S(1)} %copy-done.2), kind=kOutput, calls=%fused_computation | convolution fusion | flops 2149580800 | bytes 7340032 | tf_op jit(solution)/shard_map/sech,ehk->seck/dot_general | solution.py:279
  142.0 0.0 copy-start.8
  142.0 78.4 %giveback.1 = bf16[8,128,1024]{2,1,0:T(8,128)(2,1)} custom-call(bf16[8,128,2048]{2,1,0:T(8,128)(2,1)} %convert_bitcast_fusion.part), custom_call_target="tpu_custom_call" | custom-call | tf_op jit(solution)/shard_map/giveback/pallas_call | solution.py:282
  220.4 0.0 copy-done.8
  220.4 0.0 copy-start.6
  220.4 3.4 %convolution_convert_fusion.1 = bf16[256,1024]{1,0:T(8,128)(2,1)} fusion(bf16[1024,1024]{1,0:T(8,128)(2,1)} %bitcast.68, f32[256]{0:T(256)S(1)} %bitcast.73, s32[256]{0:T(256)S(1)} %bitcast.71, f32[256]{0:T(256)S(1)} %bitcast.72, s32[256]{0:T(256)S(1)} %bitcast.70), kind=kOutput, calls=%fused_computation.21 | convolution fusion | flops 538705920 | bytes 2625536 | tf_op jit(solution)/shard_map/dot_general | solution.py:298
  223.8 0.0 copy-done.6
  223.8 0.0 copy-start.4
  223.8 1.3 copy.38
  225.1 1.0 copy-done.4
  226.2 1.3 copy.39
  227.5 1.3 copy.40
  (10 shorter events, 0.1 us)
Async XLA Ops:
  0.6 4.3 %copy-start.7 = (s32[256,2]{0,1:T(2,128)S(1)}, s32[256,2]{0,1:T(2,128)}, u32[]{:S(2)}) copy-start(s32[256,2]{0,1:T(2,128)} %param.12) | copy-start | bytes 6148
  0.6 5.2 %copy-start = (bf16[256,2048]{1,0:T(8,128)(2,1)S(1)}, bf16[256,2048]{1,0:T(8,128)(2,1)}, u32[]{:S(2)}) copy-start(bf16[256,2048]{1,0:T(8,128)(2,1)} %param.7) | copy-start | bytes 3145732
  5.0 2.4 %copy-start.1 = (f32[8,512,128]{2,1,0:T(8,128)S(1)}, f32[8,512,128]{2,1,0:T(8,128)}, u32[]{:S(2)}) copy-start(f32[8,512,128]{2,1,0:T(8,128)} %param.11) | copy-start | bytes 6291460
  127.6 4.8 %copy-start.3 = (bf16[1,2048,512]{2,1,0:T(8,128)(2,1)S(1)}, bf16[1,2048,512]{2,1,0:T(8,128)(2,1)}, u32[]{:S(2)}) copy-start(bf16[1,2048,512]{2,1,0:T(8,128)(2,1)} %get-tuple-element.29) | copy-start | bytes 6291460
  132.4 2.4 %copy-start.5 = (bf16[1,2048,512]{2,1,0:T(8,128)(2,1)S(1)}, bf16[1,2048,512]{2,1,0:T(8,128)(2,1)}, u32[]{:S(2)}) copy-start(bf16[1,2048,512]{2,1,0:T(8,128)(2,1)} %get-tuple-element.28) | copy-start | bytes 6291460
  134.8 2.8 %copy-start.2 = (bf16[1,512,2048]{2,1,0:T(8,128)(2,1)S(1)}, bf16[1,512,2048]{2,1,0:T(8,128)(2,1)}, u32[]{:S(2)}) copy-start(bf16[1,512,2048]{2,1,0:T(8,128)(2,1)} %get-tuple-element.30) | copy-start | bytes 6291460
  142.0 78.4 %copy-start.8 = (f32[256,2]{0,1:T(2,128)S(1)}, f32[256,2]{0,1:T(2,128)}, u32[]{:S(2)}) copy-start(f32[256,2]{0,1:T(2,128)} %param.13) | copy-start | bytes 6148
  220.4 3.4 %copy-start.6 = (bf16[1,2048,512]{2,1,0:T(8,128)(2,1)S(1)}, bf16[1,2048,512]{2,1,0:T(8,128)(2,1)}, u32[]{:S(2)}) copy-start(bf16[1,2048,512]{2,1,0:T(8,128)(2,1)} %get-tuple-element.28) | copy-start | bytes 6291460
  223.8 2.3 %copy-start.4 = (bf16[1,2048,512]{2,1,0:T(8,128)(2,1)S(1)}, bf16[1,2048,512]{2,1,0:T(8,128)(2,1)}, u32[]{:S(2)}) copy-start(bf16[1,2048,512]{2,1,0:T(8,128)(2,1)} %get-tuple-element.29) | copy-start | bytes 6291460

commit v2 on v1

--- a/solution.py
+++ b/solution.py
@@ -224,6 +224,277 @@
             f_copy(k).wait_send()
 
 
+def fused_kernel(sizes, gate, up, down, rows, keys, weight, gate_hbm, up_hbm, down_hbm, mixed,
+                 gate_in, up_in, down_in, rows_in, keys_in, picked, hidden, part, held, total, back, acc,
+                 w_send, w_recv, g_send, g_recv, up_send, low_send, y_send, x_recv, t_send, t_recv, k_send, k_recv,
+                 p_send, p_recv, f_send, f_recv, own_sem, out_sem):
+    n_gr, n_fs, n_tp = sizes["gr"], sizes["fs"], sizes["tp"]
+    g, f, p = lax.axis_index("gr"), lax.axis_index("fs"), lax.axis_index("tp")
+    inner = 2 if n_fs % 2 == 0 else 1
+    lines = n_fs // inner
+    z, y = f // inner, lax.rem(f, inner)
+    depth = gate.shape[1]
+    count, width = rows.shape
+    slots = weight.shape[2]
+    half = width // n_tp
+    bf16, f32 = jnp.bfloat16, jnp.float32
+    sources, outs, finals = (gate, up, down), (gate_in, up_in, down_in), (gate_hbm, up_hbm, down_hbm)
+
+    def cols(q):
+        return pl.ds(pl.multiple_of(q * half, half), half)
+
+    def near(k):
+        return lax.rem(f + k, n_fs)
+
+    def place(w, block):
+        span = pl.ds(pl.multiple_of(block * depth, depth), depth)
+        return outs[w].at[span, :] if w < 2 else outs[w].at[:, span]
+
+    above, below, beside = {"fs": near(inner)}, {"fs": near(n_fs - inner)}, {"fs": f + 1 - 2 * y}
+
+    def block_of(b):
+        return rows_in.at[b, :, cols(p)]
+
+    def row_copy(b, first, sems, where):
+        return remote(rows.at[:, cols(p)] if first else block_of(b), block_of(b), sems.at[b], x_recv.at[b], where)
+
+    def tp_copy(b, j):
+        return remote(block_of(b), block_of(b), t_send.at[j, b], t_recv.at[j, b], {"tp": lax.rem(p + j + 1, n_tp)})
+
+    def go_up(b, first, act):
+        @pl.when(z < lines - 1)
+        def _():
+            act(row_copy(b, first, up_send, above))
+
+    def go_down(b, first, act):
+        @pl.when(z > 0)
+        def _():
+            act(row_copy(b, first, low_send, below))
+
+    def go_side(b, first, act):
+        if inner == 2:
+            act(row_copy(b, first, y_send, beside))
+
+    def start(c):
+        c.start()
+
+    def sent(c):
+        c.wait_send()
+
+    def gr_copy(w, k, j):
+        src = sources[w].at[f] if k == 0 else place(w, g * n_fs + near(n_fs - k))
+        return remote(src, place(w, g * n_fs + near(n_fs - k)), g_send.at[w, k, j], g_recv.at[w, k, j],
+                      {"gr": lax.rem(g + j + 1, n_gr)})
+
+    def w_copy(w, k):
+        to = near(k)
+        return remote(sources[w].at[to], place(w, g * n_fs + f), w_send.at[w, k], w_recv.at[w, k], {"fs": to})
+
+    def send_weights(w):
+        for k in range(1, n_fs):
+            w_copy(w, k).start()
+
+    def pass_on(w, k):
+        w_copy(w, k).wait_recv()
+        for j in range(n_gr - 1):
+            gr_copy(w, k, j).start()
+
+    def line_step(s):
+        @pl.when(z >= s)
+        def _():
+            b = f - s * inner
+            row_copy(b, False, up_send, above).wait_recv()
+            go_up(b, False, start)
+            go_side(b, False, start)
+            for j in range(n_tp - 1):
+                tp_copy(b, j).start()
+
+        @pl.when(z < lines - s)
+        def _():
+            b = f + s * inner
+            row_copy(b, False, low_send, below).wait_recv()
+            go_down(b, False, start)
+            go_side(b, False, start)
+            for j in range(n_tp - 1):
+                tp_copy(b, j).start()
+
+    def whole(w):
+        for k in range(n_fs):
+            for j in range(n_gr - 1):
+                gr_copy(w, k, j).wait_recv()
+        pltpu.make_async_copy(outs[w], finals[w].at[0], out_sem.at[w]).start()
+
+    def pick_rows(b):
+        table = keys_in[b]
+        wanted = f * slots + lax.broadcasted_iota(jnp.int32, (slots, count), 0)
+        hit = ((table[0:1, :] == wanted) | (table[1:2, :] == wanted)).astype(f32).astype(bf16)
+        for c in range(0, width, 512):
+            picked[pl.ds(pl.multiple_of(b * slots, slots), slots), c:c + 512] = jnp.dot(
+                hit, rows_in[b, :, c:c + 512], preferred_element_type=f32).astype(bf16)
+
+    greet(sizes)
+
+    own = [pltpu.make_async_copy(rows, rows_in.at[f], own_sem.at[0]),
+           pltpu.make_async_copy(keys, keys_in.at[f], own_sem.at[1])]
+    for w in range(3):
+        own.append(pltpu.make_async_copy(sources[w].at[f], place(w, g * n_fs + f), own_sem.at[2 + w]))
+
+    def key_copy(k):
+        return remote(keys, keys_in.at[f], k_send.at[k], k_recv.at[k], {"fs": near(k)})
+
+    go_up(f, True, start)
+    go_down(f, True, start)
+    go_side(f, True, start)
+    for k in range(1, n_fs):
+        key_copy(k).start()
+    for c in own:
+        c.start()
+    for w in range(3):
+        for j in range(n_gr - 1):
+            gr_copy(w, 0, j).start()
+    send_weights(0)
+    if lines > 1:
+        line_step(1)
+    send_weights(1)
+    for k in range(1, n_fs):
+        pass_on(0, k)
+    if lines > 2:
+        line_step(2)
+    send_weights(2)
+    for s in range(3, lines):
+        line_step(s)
+    if inner == 2:
+        for s in range(lines):
+            b = lax.rem(z + s, lines) * inner + 1 - y
+            row_copy(b, False, y_send, beside).wait_recv()
+            for j in range(n_tp - 1):
+                tp_copy(b, j).start()
+    for c in own:
+        c.wait()
+    pick_rows(f)
+    for k in range(1, n_fs):
+        pass_on(1, k)
+        b = near(n_fs - k)
+        for j in range(n_tp - 1):
+            tp_copy(b, j).wait_recv()
+        key_copy(k).wait_recv()
+        pick_rows(b)
+    whole(0)
+    whole(1)
+    group = 2 if n_fs % 2 == 0 else 1
+    for i in range(n_fs // group):
+        for k in range(1 + i * group, min(1 + (i + 1) * group, n_fs)):
+            pass_on(2, k)
+        span = slice(i * group * slots, (i + 1) * group * slots)
+        gate_act = jnp.dot(picked[span, :], gate_in[...], preferred_element_type=f32)
+        up_act = jnp.dot(picked[span, :], up_in[...], preferred_element_type=f32)
+        hidden[span, :] = (gate_act / (1.0 + jnp.exp(-gate_act)) * up_act).astype(bf16)
+    whole(2)
+
+    order = list(range(1, n_fs)) + [0]
+
+    def p_copy(k, j):
+        to = lax.rem(p + j + 1, n_tp)
+        b = near(k)
+        return remote(part.at[b, :, cols(to)], held.at[j, b], p_send.at[j, k], p_recv.at[j, k], {"tp": to})
+
+    def f_copy(k):
+        return remote(total.at[near(k)], back.at[f], f_send.at[k], f_recv.at[k], {"fs": near(k)})
+
+    for i in range(n_fs + 3):
+        if i < n_fs:
+            b = near(order[i])
+            mine = hidden[pl.ds(pl.multiple_of(b * slots, slots), slots), :]
+            for c in range(0, width, 512):
+                part[b, :, c:c + 512] = jnp.dot(mine, down_in[:, c:c + 512], preferred_element_type=f32).astype(bf16)
+        if 0 <= i - 1 < n_fs:
+            for j in range(n_tp - 1):
+                p_copy(order[i - 1], j).start()
+        if 0 <= i - 2 < n_fs:
+            k = order[i - 2]
+            b = near(k)
+            value = part[b, :, cols(p)].astype(f32)
+            for j in range(n_tp - 1):
+                p_copy(k, j).wait_recv()
+                value = value + held[j, b].astype(f32)
+            total[b] = value.astype(bf16)
+        if 0 <= i - 3 < n_fs and order[i - 3]:
+            f_copy(order[i - 3]).start()
+
+    acc[...] = jnp.dot(weight[f], total[f], preferred_element_type=f32)
+    for k in range(1, n_fs):
+        f_copy(k).wait_recv()
+        b = near(n_fs - k)
+        acc[...] += jnp.dot(weight[b], back[b], preferred_element_type=f32)
+    mixed[...] = acc[...].astype(bf16)
+
+    for k in range(n_fs):
+        for j in range(n_tp - 1):
+            p_copy(k, j).wait_send()
+        if k:
+            f_copy(k).wait_send()
+            key_copy(k).wait_send()
+            for j in range(n_tp - 1):
+                tp_copy(near(k), j).wait_send()
+        for w in range(3):
+            if k:
+                w_copy(w, k).wait_send()
+            for j in range(n_gr - 1):
+                gr_copy(w, k, j).wait_send()
+    go_up(f, True, sent)
+    go_down(f, True, sent)
+    go_side(f, True, sent)
+    for s in range(1, lines):
+        @pl.when(z >= s)
+        def _():
+            go_up(f - s * inner, False, sent)
+            go_side(f - s * inner, False, sent)
+
+        @pl.when(z < lines - s)
+        def _():
+            go_down(f + s * inner, False, sent)
+            go_side(f + s * inner, False, sent)
+    for w in range(3):
+        pltpu.make_async_copy(outs[w], finals[w].at[0], out_sem.at[w]).wait()
+
+
+def run_fused(sizes, gate_cast, up_cast, down_cast, normed, keys, weight):
+    n_gr, n_fs, n_tp = sizes["gr"], sizes["fs"], sizes["tp"]
+    _, depth, hid = gate_cast.shape
+    count, width = normed.shape
+    slots = weight.shape[2]
+    half = width // n_tp
+    bf16, dma = jnp.bfloat16, pltpu.SemaphoreType.DMA
+    vmem = pl.BlockSpec(memory_space=pltpu.VMEM)
+    return pl.pallas_call(
+        functools.partial(fused_kernel, sizes),
+        out_shape=(
+            jax.ShapeDtypeStruct((1, n_gr * n_fs * depth, hid), bf16),
+            jax.ShapeDtypeStruct((1, n_gr * n_fs * depth, hid), bf16),
+            jax.ShapeDtypeStruct((1, hid, n_gr * n_fs * depth), bf16),
+            jax.ShapeDtypeStruct((count, half), bf16),
+        ),
+        in_specs=[vmem] * 6,
+        out_specs=[pl.BlockSpec(memory_space=pl.ANY)] * 3 + [vmem],
+        scratch_shapes=[
+            pltpu.VMEM((n_gr * n_fs * depth, hid), bf16), pltpu.VMEM((n_gr * n_fs * depth, hid), bf16),
+            pltpu.VMEM((hid, n_gr * n_fs * depth), bf16),
+            pltpu.VMEM((n_fs, count, width), bf16), pltpu.VMEM((n_fs, 8, count), jnp.int32),
+            pltpu.VMEM((n_fs * slots, width), bf16), pltpu.VMEM((n_fs * slots, hid), bf16),
+            pltpu.VMEM((n_fs, slots, width), bf16),
+            pltpu.VMEM((max(n_tp - 1, 1), n_fs, slots, half), bf16),
+            pltpu.VMEM((n_fs, slots, half), bf16), pltpu.VMEM((n_fs, slots, half), bf16),
+            pltpu.VMEM((count, half), jnp.float32),
+            dma((3, n_fs)), dma((3, n_fs)), dma((3, n_fs, n_gr)), dma((3, n_fs, n_gr)),
+            dma((n_fs,)), dma((n_fs,)), dma((n_fs,)), dma((n_fs,)),
+            dma((n_tp, n_fs)), dma((n_tp, n_fs)), dma((n_fs,)), dma((n_fs,)),
+            dma((n_tp, n_fs)), dma((n_tp, n_fs)), dma((n_fs,)), dma((n_fs,)), dma((5,)), dma((3,)),
+        ],
+        compiler_params=pltpu.CompilerParams(collective_id=2, has_side_effects=True, vmem_limit_bytes=62 * 2**20),
+        name="handover",
+    )(gate_cast, up_cast, down_cast, normed, keys, weight)
+
+
 def on_device(sizes, tokens, norm_gain, gate_train, up_train, down_train, expert_ids, route_score):
     n_gr, n_fs, n_tp = sizes["gr"], sizes["fs"], sizes["tp"]
     bf16 = jnp.bfloat16
@@ -244,7 +515,13 @@
     slot = expert_ids * capacity + jnp.sum(jnp.where(named, rank[:, None, :], 0), axis=2)
     keys = jnp.concatenate([slot.T, jnp.full((6, count), -1, jnp.int32)], axis=0)
 
+    share = route_score / jnp.sum(route_score, axis=-1, keepdims=True)
     direct_down = depth % 128 == 0
+    if direct_down and local == 1 and capacity % 128 == 0:
+        at = (jnp.arange(experts, dtype=jnp.int32)[:, None] * capacity + jnp.arange(capacity, dtype=jnp.int32))[:, None, :]
+        weight = jnp.where(slot[None, :, :1] == at, share[None, :, :1], 0.0) + jnp.where(slot[None, :, 1:] == at, share[None, :, 1:], 0.0)
+        return run_fused(sizes, gate_cast, up_cast, down_cast, normed, keys, weight.astype(bf16))
+
     down_shape = (local, hid, n_gr * n_fs * depth) if direct_down else (n_gr * n_fs, local, hid, depth)
     dma = pltpu.SemaphoreType.DMA
     gate_ready, up_ready, down_ready, gathered, all_keys = pl.pallas_call(
@@ -292,7 +569,6 @@
         compiler_params=pltpu.CompilerParams(collective_id=1, has_side_effects=True),
         name="giveback",
     )(part)
-    share = route_score / jnp.sum(route_score, axis=-1, keepdims=True)
     at = jnp.arange(experts * capacity, dtype=jnp.int32)[None, :]
     weight = jnp.where(slot[:, :1] == at, share[:, :1], 0.0) + jnp.where(slot[:, 1:] == at, share[:, 1:], 0.0)
     mixed = jnp.dot(weight.astype(bf16), returned.reshape(experts * capacity, half), preferred_element_type=jnp.float32)

time: 229 us -> 220 us (0.961)
  the two profiles are of different devices: /device:TPU:13 before, /device:TPU:0 now
where the time goes in v2:
time: 220 us
  Pallas kernels  198 us (90%)
  other arithmetic  12.4 us (6%)
  local copies, waits for them, and re-layouts  8.36 us (4%)
    pallas_call x1, Pallas kernels, run_fused(): pl.pallas_call(functools.partial(fused_kernel, sizes), out_shape=(jax.Sha...  198 us
    unnamed x18, local copies, waits for them, and re-layouts  7.75 us

profile of v2, /device:TPU:0, one launch (start us, length us, event | category | flops | bytes accessed | tf_op | source)
XLA Modules:
  0.0 219.6 jit_solution(17364928643108247474)
XLA Ops:
  0.6 0.0 copy-start
  0.7 1.6 fusion
  2.3 0.7 reduce_sum.29
  3.0 0.7 broadcast_divide_fusion
  3.7 0.7 fusion.2
  4.3 0.1 iota_add_fusion
  4.4 0.2 convolution_convert_fusion
  4.6 0.7 select_reduce_fusion
  5.3 0.7 multiply_add_fusion
  6.0 0.6 concatenate.3.keys
  6.6 1.1 add_convert_fusion.weight
  7.7 0.0 copy-done
  7.7 0.0 copy-start.2
  7.7 1.2 fusion.1.rows
  8.9 0.0 copy-start.1
  8.9 0.0 copy-start.6
  8.9 2.9 %convert_element_type.25.down = bf16[8,512,128]{2,1,0:T(8,128)(2,1)} convert(f32[8,512,128]{2,1,0:T(8,128)} %param.11) | non-fusion elementwise | flops 524288 | bytes 3145728 | tf_op jit(solution)/shard_map/convert_element_type | solution.py:507
  11.8 0.0 copy-done.2
  11.8 0.0 copy-done.1
  11.8 0.0 copy-done.6
  11.8 2.0 multiply_convert_fusion
  13.8 198.0 %handover.1 = (bf16[1,2048,512]{2,1,0:T(8,128)(2,1)}, bf16[1,2048,512]{2,1,0:T(8,128)(2,1)}, bf16[1,512,2048]{2,1,0:T(8,128)(2,1)}, bf16[256,1024]{1,0:T(8,128)(2,1)}) custom-call(bf16[8,128,512]{2,1,0:T(8,128)(2,1)} %get-tuple-element.9.gate, bf16[8,128,512]{2,1,0:T(8,128)(2,1)} %get-tuple-element.8.up, bf16[8,512,128]{2,1,0:T(8,128)(2,1)} %convert_element_type.25.down, ...), custom_call_target="tpu_custom_call" | custom-call | tf_op jit(solution)/shard_map/handover/pallas_call | solution.py:469
  211.9 0.0 copy-start.4
  211.9 3.2 %copy.17 = bf16[1,2048,512]{2,1,0:T(8,128)(2,1)} copy(bf16[1,2048,512]{2,1,0:T(8,128)(2,1)} %get-tuple-element.14) | data formatting | bytes 4194304
  215.1 0.0 copy-done.4
  215.1 0.0 copy-start.3
  215.1 1.3 copy.18
  216.4 1.0 copy-done.3
  217.4 0.0 copy-start.5
  217.4 1.3 copy.19
  218.8 0.1 copy-done.5
  218.8 0.8 copy.20
  (4 shorter events, 0.0 us)
Async XLA Ops:
  0.6 7.0 %copy-start = (bf16[256,2048]{1,0:T(8,128)(2,1)S(1)}, bf16[256,2048]{1,0:T(8,128)(2,1)}, u32[]{:S(2)}) copy-start(bf16[256,2048]{1,0:T(8,128)(2,1)} %param.7) | copy-start | bytes 3145732
  7.7 4.1 %copy-start.2 = (f32[8,128,512]{2,1,0:T(8,128)S(1)}, f32[8,128,512]{2,1,0:T(8,128)}, u32[]{:S(2)}) copy-start(f32[8,128,512]{2,1,0:T(8,128)} %param.9) | copy-start | bytes 6291460
  8.9 2.9 %copy-start.1 = (f32[8,128,512]{2,1,0:T(8,128)S(1)}, f32[8,128,512]{2,1,0:T(8,128)}, u32[]{:S(2)}) copy-start(f32[8,128,512]{2,1,0:T(8,128)} %param.10) | copy-start | bytes 6291460
  8.9 2.9 %copy-start.6 = (f32[128]{0:T(128)S(1)}, f32[128]{0:T(128)}, u32[]{:S(2)}) copy-start(f32[128]{0:T(128)} %param.8) | copy-start | bytes 1540
  211.9 3.2 %copy-start.4 = (bf16[1,2048,512]{2,1,0:T(8,128)(2,1)S(1)}, bf16[1,2048,512]{2,1,0:T(8,128)(2,1)}, u32[]{:S(2)}) copy-start(bf16[1,2048,512]{2,1,0:T(8,128)(2,1)} %get-tuple-element.15) | copy-start | bytes 6291460
  215.1 2.3 %copy-start.3 = (bf16[1,512,2048]{2,1,0:T(8,128)(2,1)S(1)}, bf16[1,512,2048]{2,1,0:T(8,128)(2,1)}, u32[]{:S(2)}) copy-start(bf16[1,512,2048]{2,1,0:T(8,128)(2,1)} %get-tuple-element.16) | copy-start | bytes 6291460
  217.4 1.4 copy-start.5
